TPU v7x, 32 devices: a whole 2x2x4 slice. The times are simulated.
32 devices in a mesh: grp: 2 (over y), sp: 4 (over z), tp: 4 (over x, core).
Axes of the slice: x: 2, y: 2, z: 4, core: 2. Of those that a mesh axis runs over, the one named last changes fastest.
Arguments:
- latents: bfloat16 [2048, 4, 2048], P(('sp', 'tp'), 'grp'), parts along dimension 1, may hold values from -6 to 6
- context: bfloat16 [1024, 4, 2048], P('sp', 'grp'), parts along dimension 1, may hold values from -6 to 6
- condition: float32 [4, 2048], P('grp', 'sp'), parts along dimension 0, may hold values from -6 to 6
- cond_context: float32 [2048], P('sp'), may hold values from -6 to 6
- w_shift: bfloat16 [2048, 2048], P('sp', 'tp'), may hold values from -0.125 to 0.125
- w_scale: bfloat16 [2048, 2048], P('sp', 'tp'), may hold values from -0.125 to 0.125
- w_gate: bfloat16 [2048, 2048], P('sp', 'tp'), may hold values from -0.375 to 0.375
- norm_gain: float32 [2048], replicated, may hold values from 0.1 to 1.9
- w_query: bfloat16 [2048, 1024], P(None, 'tp'), may hold values from -0.375 to 0.375
- w_key: bfloat16 [2048, 512], P(None, 'tp'), may hold values from -0.125 to 0.125
- w_value: bfloat16 [2048, 512], P(None, 'tp'), may hold values from -0.25 to 0.25
- sink_logit: float32 [16], P('tp'), may hold values from 6 to 240
- w_out: bfloat16 [1024, 2048], P('tp'), may hold values from -0.1875 to 0.1875
Outputs:
- refined: bfloat16 [2048, 4, 2048], P(('sp', 'tp'), 'grp'), parts along dimension 1
There are 2 independent parts, one for each index of `grp`. A program takes and returns all parts, laid end to end along the dimension named above; an argument that names none is the same for every part. Nothing has to cross between parts.
All inputs are finite; a program needn't handle non-finite values.
Results may differ from a plain program's by a relative error of at most 0.017.
Values may be sent and summed in bfloat16 or wider, within the bound.
No kernel may reach another device: no remote copies, remote signals or barrier semaphores. Data moves between devices by JAX's collectives and lax.ppermute only.
A program may use at most 128 MiB of HBM per device.

v0:
```python
import jax
import jax.numpy as jnp
from jax import lax
from jax.sharding import PartitionSpec as P

HEAD_DIM = 64
WINDOW = 128
GRID_W = 64
EPS = 1e-06
THETA = 10000.0
BIG_NEG = -1e30


def with_halo(cells, sides, width):
    for axis, dim in sides:
        count = lax.axis_size(axis)
        ends = count - 1
        head = lax.slice_in_dim(cells, 0, width, axis=dim)
        tail = lax.slice_in_dim(cells, cells.shape[dim] - width, cells.shape[dim], axis=dim)
        cells = jnp.concatenate(
            [
                lax.ppermute(tail, axis, [(i, (i + 1) % count) for i in range(ends)]),
                cells,
                lax.ppermute(head, axis, [((i + 1) % count, i) for i in range(ends)]),
            ],
            axis=dim,
        )
    return cells


def rotate_pairs(vectors, grid_row, grid_col, head_dim):
    quarter = head_dim // 4
    inverse = THETA ** (-jnp.arange(quarter, dtype=jnp.float32) / quarter)
    angles = jnp.concatenate([grid_row[:, None] * inverse, grid_col[:, None] * inverse], axis=-1)
    shape = (angles.shape[0],) + (1,) * (vectors.ndim - 2) + (head_dim // 2,)
    cosine = jnp.cos(angles).reshape(shape)
    sine = jnp.sin(angles).reshape(shape)
    first_half = vectors[..., : head_dim // 2]
    second_half = vectors[..., head_dim // 2 :]
    return jnp.concatenate(
        [first_half * cosine - second_half * sine, first_half * sine + second_half * cosine],
        axis=-1,
    )


def modulate(tokens_in, gain, shift_rows, scale_rows):
    upcast = tokens_in.astype(jnp.float32)
    normed = upcast * lax.rsqrt(jnp.mean(upcast * upcast, axis=-1, keepdims=True) + EPS)
    return (normed * gain * (1.0 + scale_rows) + shift_rows).astype(jnp.bfloat16)


def on_device(
    latents,
    context,
    condition,
    cond_context,
    w_shift,
    w_scale,
    w_gate,
    norm_gain,
    w_query,
    w_key,
    w_value,
    sink_logit,
    w_out,
):
    samples = latents.shape[1]
    model_width = latents.shape[2]
    n_tp = lax.axis_size("tp")
    n_sp = lax.axis_size("sp")
    local_rows = latents.shape[0]
    tokens = local_rows * n_tp
    local_heads = w_query.shape[1] // HEAD_DIM
    local_kv = w_key.shape[1] // HEAD_DIM
    per_group = local_heads // local_kv
    q_cols = local_heads * HEAD_DIM
    kv_cols = local_kv * HEAD_DIM
    lifted = jax.nn.silu(jnp.concatenate([condition, cond_context[None, :]], axis=0)).astype(
        jnp.bfloat16
    )
    part_shift = jnp.dot(lifted, w_shift, preferred_element_type=jnp.float32)
    part_scale = jnp.dot(lifted, w_scale, preferred_element_type=jnp.float32)
    part_gate = jnp.dot(lifted, w_gate, preferred_element_type=jnp.float32)
    sum_shift, sum_scale, sum_gate = lax.psum((part_shift, part_scale, part_gate), "sp")
    shift_all, scale_all, gate_all = (
        lax.all_gather(sum_shift, "tp", axis=1, tiled=True),
        lax.all_gather(sum_scale, "tp", axis=1, tiled=True),
        lax.all_gather(sum_gate, "tp", axis=1, tiled=True),
    )
    normed = modulate(latents, norm_gain, shift_all[:samples][None], scale_all[:samples][None])
    w_joint = jnp.concatenate([w_query, w_key, w_value], axis=1)
    shard_rows = lax.all_gather(normed, "tp", axis=0, tiled=True)
    row_count = shard_rows.shape[0]
    flat_rows = shard_rows.reshape(row_count * samples, model_width)
    projected = jnp.dot(flat_rows, w_joint, preferred_element_type=jnp.float32).reshape(
        row_count, samples, w_joint.shape[1]
    )
    offset = lax.axis_index("sp") * tokens
    positions = offset + jnp.arange(tokens, dtype=jnp.int32)
    grid_row = (positions // GRID_W).astype(jnp.float32)
    grid_col = (positions % GRID_W).astype(jnp.float32)
    queries = rotate_pairs(
        projected[..., :q_cols].reshape(tokens, samples, local_heads, HEAD_DIM),
        grid_row,
        grid_col,
        HEAD_DIM,
    ).astype(jnp.bfloat16)
    lat_keys = rotate_pairs(
        projected[..., q_cols : q_cols + kv_cols].reshape(tokens, samples, local_kv, HEAD_DIM),
        grid_row,
        grid_col,
        HEAD_DIM,
    ).astype(jnp.bfloat16)
    lat_values = projected[..., q_cols + kv_cols :].astype(jnp.bfloat16)
    paired = jnp.concatenate([lat_keys.reshape(tokens, samples, kv_cols), lat_values], axis=-1)
    extended = with_halo(paired, (("sp", 0),), WINDOW)
    w_pair = jnp.concatenate([w_key, w_value], axis=1)
    ctx_shift = shift_all[samples][None, None]
    ctx_scale = scale_all[samples][None, None]
    ctx_normed = modulate(context, norm_gain, ctx_shift, ctx_scale)
    row_count = context.shape[0]
    flat_ctx = ctx_normed.reshape(row_count * samples, model_width)
    ctx_pairs = lax.all_gather(
        jnp.dot(flat_ctx, w_pair, preferred_element_type=jnp.float32)
        .astype(jnp.bfloat16)
        .reshape(row_count, samples, 2 * kv_cols),
        "sp",
        axis=0,
        tiled=True,
    )
    ctx_len = ctx_pairs.shape[0]
    ctx_keys = ctx_pairs[..., :kv_cols].reshape(ctx_len, samples, local_kv, HEAD_DIM)
    ctx_values = ctx_pairs[..., kv_cols:].reshape(ctx_len, samples, local_kv, HEAD_DIM)
    block_rows = min(tokens, 512)
    n_blocks = tokens // block_rows
    seq_length = tokens * n_sp
    head_sinks = sink_logit.reshape(local_kv, per_group)[None, :, :, None]
    score_scale = HEAD_DIM ** (-0.5)

    def attend_block(block_index):
        first_row = block_index * block_rows
        q_blk = queries.reshape(block_rows, samples, local_kv, per_group, HEAD_DIM)
        k_blk = extended[..., :kv_cols].reshape(
            block_rows + 2 * WINDOW, samples, local_kv, HEAD_DIM
        )
        v_blk = extended[..., kv_cols:].reshape(
            block_rows + 2 * WINDOW, samples, local_kv, HEAD_DIM
        )
        lat_scores = (
            jnp.einsum("qsngd,ksnd->sngqk", q_blk, k_blk, preferred_element_type=jnp.float32)
            * score_scale
        )
        q_pos = offset + first_row + jnp.arange(block_rows, dtype=jnp.int32)
        k_pos = offset + first_row - WINDOW + jnp.arange(block_rows + 2 * WINDOW, dtype=jnp.int32)
        in_window = (
            (jnp.abs(q_pos[:, None] - k_pos[None, :]) <= WINDOW)
            & (k_pos >= 0)[None, :]
            & (k_pos < seq_length)[None, :]
        )
        lat_scores = jnp.where(in_window, lat_scores, BIG_NEG)
        ctx_scores = (
            jnp.einsum("qsngd,ksnd->sngqk", q_blk, ctx_keys, preferred_element_type=jnp.float32)
            * score_scale
        )
        row_max = jnp.maximum(
            jnp.maximum(jnp.max(lat_scores, axis=-1), jnp.max(ctx_scores, axis=-1)), head_sinks
        )
        lat_exp = jnp.exp(lat_scores - row_max[..., None])
        ctx_exp = jnp.exp(ctx_scores - row_max[..., None])
        denominator = (
            jnp.sum(lat_exp, axis=-1) + jnp.sum(ctx_exp, axis=-1) + jnp.exp(head_sinks - row_max)
        )
        lat_weights = (lat_exp / denominator[..., None]).astype(jnp.bfloat16)
        ctx_weights = (ctx_exp / denominator[..., None]).astype(jnp.bfloat16)
        summed = jnp.einsum(
            "sngqk,ksnd->qsngd", lat_weights, v_blk, preferred_element_type=jnp.float32
        )
        summed = summed + jnp.einsum(
            "sngqk,ksnd->qsngd", ctx_weights, ctx_values, preferred_element_type=jnp.float32
        )
        return summed.astype(jnp.bfloat16).reshape(block_rows, samples, q_cols)

    attended = lax.map(attend_block, jnp.arange(n_blocks)).reshape(tokens * samples, q_cols)
    summed_out = lax.psum_scatter(
        jnp.dot(attended, w_out, preferred_element_type=jnp.float32).astype(jnp.bfloat16),
        "tp",
        scatter_dimension=0,
        tiled=True,
    ).astype(jnp.float32)
    mixed = summed_out.reshape(local_rows, samples, model_width)
    refined = latents.astype(jnp.float32) + gate_all[:samples][None] * mixed
    return refined.astype(jnp.bfloat16)


def solution(mesh):
    return jax.shard_map(
        on_device,
        mesh=mesh,
        in_specs=(
            P(("sp", "tp"), "grp", None),
            P("sp", "grp", None),
            P("grp", "sp"),
            P("sp"),
            P("sp", "tp"),
            P("sp", "tp"),
            P("sp", "tp"),
            P(),
            P(None, "tp"),
            P(None, "tp"),
            P(None, "tp"),
            P("tp"),
            P("tp", None),
        ),
        out_specs=P(("sp", "tp"), "grp", None),
        check_vma=False,
    )
```

profile of v0, /device:TPU:0, one launch (start us, length us, event | category | flops | bytes accessed | tf_op | source)
XLA Modules:
  0.0 237.9 jit_solution(7936242793611745387)
XLA Ops:
  6.5 1.4 fusion.49
  10.5 20.7 %all-reduce = (f32[3,512]{1,0:T(4,128)S(1)}, f32[3,512]{1,0:T(4,128)S(1)}, f32[3,512]{1,0:T(4,128)S(1)}) all-reduce(f32[3,512]{1,0:T(4,128)S(1)} %fusion.49, f32[3,512]{1,0:T(4,128)S(1)} %fusion.51, f32[3,512]{1,0:T(4,128)S(1)} %fusion.53), channel_id=1, replica_groups=mesh['grp'=2,'sp'=4,'tp'=4] {'sp'}, use_global_device_ids=true, to_apply=%region_3.4 | all-reduce | flops 4608 | bytes 36864 | tf_op jit(solution)/shard_map/psum | solution.py:84
  31.1 5.2 %all_gather.17 = f32[3,2048]{1,0:T(4,128)S(1)} all-gather(f32[3,512]{1,0:T(4,128)S(1)} %get-tuple-element.19), channel_id=1, replica_groups=mesh['grp'=2,'sp'=4,'tp'=4] {'tp'}, dimensions={1}, use_global_device_ids=true | all-gather | bytes 30720 | tf_op jit(solution)/shard_map/all_gather | solution.py:86
  36.3 5.2 %all_gather.16 = f32[3,2048]{1,0:T(4,128)S(1)} all-gather(f32[3,512]{1,0:T(4,128)S(1)} %get-tuple-element.20), channel_id=1, replica_groups=mesh['grp'=2,'sp'=4,'tp'=4] {'tp'}, dimensions={1}, use_global_device_ids=true | all-gather | bytes 30720 | tf_op jit(solution)/shard_map/all_gather | solution.py:87
  41.5 3.8 %fusion.6 = f32[256,2]{1,0:T(8,128)S(1)} fusion(bf16[256,2,2048]{2,1,0:T(2,128)(2,1)} %param.14), kind=kLoop, calls=%fused_computation.14 | loop fusion | flops 3145216 | bytes 2099200 | tf_op jit(solution)/shard_map/reduce_sum | solution.py:48
  45.4 4.5 %fusion.10 = bf16[256,2,2048]{2,1,0:T(2,128)(2,1)} fusion(bf16[256,2,2048]{2,1,0:T(2,128)(2,1)S(1)} %copy-done.3, f32[2048]{0:T(1024)S(1)} %bitcast.83, f32[2048]{0:T(1024)S(1)} %bitcast.84, f32[2048]{0:T(1024)S(1)} %copy-done.6, f32[256,2]{1,0:T(8,128)S(1)} %add_rsqrt_fusion), kind=kLoop, calls=%fused_computation.18 | loop fusion | flops 6291456 | bytes 4220928 | tf_op jit(solution)/shard_map/convert_element_type | solution.py:49
  50.0 4.2 %reshape.218 = bf16[512,2048]{1,0:T(8,128)(2,1)} reshape(bf16[256,2,2048]{2,1,0:T(2,128)(2,1)} %fusion.10) | data formatting | bytes 4194304 | tf_op jit(solution)/shard_map/reshape | solution.py:122
  54.2 2.4 %convolution_convert_fusion.1 = bf16[512,256]{1,0:T(8,128)(2,1)S(1)} fusion(bf16[512,2048]{1,0:T(8,128)(2,1)} %reshape.218, bf16[2048,128]{1,0:T(8,128)(2,1)S(1)} %copy-done.4, bf16[2048,128]{1,0:T(8,128)(2,1)} %param.22), kind=kOutput, calls=%fused_computation.42 | convolution fusion | flops 539099136 | bytes 3407872 | tf_op jit(solution)/shard_map/dot_general | solution.py:124
  57.9 1.6 fusion.15
  60.6 2.0 copy.59
  62.6 2.3 copy.58
  66.2 17.6 %all-gather.5.cloned.1.call-done = bf16[1024,2,256]{2,1,0:T(2,128)(2,1)} async-done(((bf16[256,2,256]{2,1,0:T(2,128)(2,1)}), bf16[1024,2,256]{2,1,0:T(2,128)(2,1)}) %all-gather.5.cloned.1.call-update) | async-done | bytes 1048592 | tf_op jit(solution)/shard_map/all_gather | solution.py:123
  83.8 2.7 %fusion.55 = (bf16[1024,2,128]{2,1,0:T(2,128)(2,1)}, bf16[1024,2,128]{2,1,0:T(2,128)(2,1)S(1)}) fusion(bf16[1024,2,256]{2,1,0:T(2,128)(2,1)} %all-gather.5.cloned.1.call-done), kind=kLoop, calls=%fused_computation.98 | loop fusion | bytes 2097152 | tf_op jit(solution)/shard_map/slice | solution.py:132
  87.6 1.3 copy.63
  88.9 30.3 %all-gather.3.cloned.1.call-done = bf16[512,2,2048]{2,0,1:T(8,128)(2,1)} async-done(((bf16[128,2,2048]{2,0,1:T(8,128)(2,1)}), bf16[512,2,2048]{2,0,1:T(8,128)(2,1)}) %all-gather.3.cloned.1.call-update) | async-done | bytes 4194320 | tf_op jit(solution)/shard_map/all_gather | solution.py:92
  119.2 5.2 %fusion.17 = f32[512,2,512]{0,2,1:T(8,128)S(1)} fusion(bf16[512,2,2048]{2,0,1:T(8,128)(2,1)} %all-gather.3.cloned.1.call-done, bf16[2048,128]{0,1:T(8,128)(2,1)} %copy.60, bf16[2048,128]{0,1:T(8,128)(2,1)} %copy.59, bf16[2048,256]{0,1:T(8,128)(2,1)} %copy.58), kind=kOutput, calls=%fused_computation.30 | convolution fusion | flops 2153775104 | bytes 8388608 | tf_op jit(solution)/shard_map/dot_general | solution.py:95
  126.2 4.7 %collective-permute-start = (bf16[128,2,256]{0,2,1:T(8,128)(2,1)S(1)}, bf16[128,2,256]{0,2,1:T(8,128)(2,1)S(1)}, u32[]{:S(2)}, u32[]{:S(2)}) collective-permute-start(bf16[128,2,256]{0,2,1:T(8,128)(2,1)S(1)} %get-tuple-element.40), channel_id=1, source_target_pairs={{0,4},{4,8},{8,12},{1,5},{5,9},{9,13},{2,6},{6,10},{10,14},{3,7},{... | collective-permute-start | bytes 393224 | tf_op jit(solution)/shard_map/ppermute | solution.py:22
  130.9 8.1 %bitcast_reduce_fusion = (f32[2,2,2,512]{3,2,1,0:T(2,128)S(1)}, f32[2,2,1024,512,2]{3,2,4,1,0:T(8,128)}) fusion(bf16[1024,2,2,64,1]{0,3,4,2,1:T(8,128)(2,1)S(1)} %bitcast.74, bf16[512,2,2,2,32]{0,4,3,2,1:T(8,128)(2,1)S(1)} %bitcast.78, bf16[512,2,2,2,32]{0,4,3,2,1:T(8,128)(2,1)S(1)} %bitcast.76), kind=kOutput, calls=%fused_computation.1 | convolution fusion | flops 546304000 | bytes 17842176 | tf_op jit(solution)/shard_map/while/body/eval_jaxpr/qsngd,ksnd->sngqk/dot_general | solution.py:162
  139.9 2.1 fusion.3
  142.2 2.6 %fusion.2 = f32[2,2,2,512]{3,2,1,0:T(2,128)S(1)} fusion(f32[2,2,768,512,2]{3,2,4,1,0:T(8,128)S(1)} %get-tuple-element.47, f32[2,2,2,512]{3,2,1,0:T(2,128)S(1)} %maximum_maximum_fusion, pred[512,768]{0,1:T(8,128)(4,1)S(1)} %fusion.23), kind=kLoop, calls=%fused_computation.8 | loop fusion | flops 12578816 | bytes 13008896 | tf_op jit(solution)/shard_map/while/body/eval_jaxpr/reduce_sum | solution.py:171
  144.8 1.8 copy-done.1
  146.6 9.3 %fusion.1 = f32[2,2,2,512]{3,2,1,0:T(2,128)} fusion(f32[2,2,1024,512,2]{3,2,4,1,0:T(8,128)} %get-tuple-element.49, f32[2,2,2,512]{3,2,1,0:T(2,128)S(1)} %maximum_maximum_fusion), kind=kLoop, calls=%fused_computation.4 | loop fusion | flops 12578816 | bytes 16809984 | tf_op jit(solution)/shard_map/while/body/eval_jaxpr/reduce_sum | solution.py:171
  156.8 8.0 %fusion.4 = f32[2,2,64,2,512]{4,2,3,1,0:T(8,128)S(1)} fusion(bf16[1024,2,2,64,1]{0,3,4,2,1:T(8,128)(2,1)} %bitcast.80, f32[2,2,1024,512,2]{3,2,4,1,0:T(8,128)} %get-tuple-element.49, f32[2,2,2,512]{3,2,1,0:T(2,128)S(1)} %exponential_add_fusion, f32[2,2,2,512]{3,2,1,0:T(2,128)S(1)} %maximum_maximum_fusion), kind=kOutput, calls=%fused_computation.10 | convolution fusion | flops 553648128 | bytes 18382848 | tf_op jit(solution)/shard_map/while/body/eval_jaxpr/sngqk,ksnd->qsngd/dot_general | solution.py:178
  165.3 4.3 %fusion.26 = bf16[512,2,2,2,64]{0,4,3,2,1:T(8,128)(2,1)} fusion(f32[2,2,64,2,512]{4,2,3,1,0:T(8,128)S(1)} %fusion.4, bf16[768,2,2,64,1]{0,3,4,2,1:T(8,128)(2,1)S(1)} %bitcast.81, f32[2,2,768,512,2]{3,2,4,1,0:T(8,128)S(1)} %bitcast.70, f32[2,2,2,512]{3,2,1,0:T(2,128)S(1)} %exponential_add_fusion, f32[2,2,2,512]{3,2,1,0:T(2,128)S(1)} %maximum_maximum_fusion, ...), kind=kOutput, calls=%fused_computation.41 | convolution fusion | flops 418906112 | bytes 14974976 | tf_op jit(solution)/shard_map/while/body/eval_jaxpr/sngqk,ksnd->qsngd/dot_general | solution.py:175
  169.6 3.6 %copy.67 = bf16[512,2,2,2,64]{4,3,2,1,0:T(2,128)(2,1)} copy(bf16[512,2,2,2,64]{0,4,3,2,1:T(8,128)(2,1)} %fusion.26) | data formatting | bytes 1048576 | tf_op jit(solution)/shard_map/while/body/eval_jaxpr/convert_element_type | solution.py:181
  173.1 2.8 %reshape.222 = bf16[1024,256]{1,0:T(8,128)(2,1)S(1)} reshape(bf16[512,2,2,2,64]{4,3,2,1,0:T(2,128)(2,1)} %copy.67) | data formatting | bytes 1048576 | tf_op jit(solution)/shard_map/reshape | solution.py:183
  175.9 3.2 %convolution_convert_fusion = bf16[1024,2048]{1,0:T(8,128)(2,1)} fusion(bf16[1024,256]{1,0:T(8,128)(2,1)S(1)} %reshape.222, bf16[256,2048]{1,0:T(8,128)(2,1)S(1)} %copy-done), kind=kOutput, calls=%fused_computation.19 | convolution fusion | flops 1075838976 | bytes 5767168 | tf_op jit(solution)/shard_map/dot_general | solution.py:185
  179.1 5.2 %all_gather.15 = f32[3,2048]{1,0:T(4,128)S(1)} all-gather(f32[3,512]{1,0:T(4,128)S(1)} %get-tuple-element.21), channel_id=1, replica_groups=mesh['grp'=2,'sp'=4,'tp'=4] {'tp'}, dimensions={1}, use_global_device_ids=true | all-gather | bytes 30720 | tf_op jit(solution)/shard_map/all_gather | solution.py:88
  184.3 38.6 %reduce-scatter.2.cloned.1.call-done = bf16[256,2048]{1,0:T(8,128)(2,1)} async-done(((bf16[1024,2048]{1,0:T(8,128)(2,1)}), bf16[256,2048]{1,0:T(8,128)(2,1)}) %reduce-scatter.2.cloned.1.call-update) | async-done | bytes 1048592 | tf_op jit(solution)/shard_map/reduce_scatter | solution.py:184
  223.0 3.4 %reshape.226 = f32[128,2,2048]{2,1,0:T(2,128)} reshape(bf16[256,2048]{1,0:T(8,128)(2,1)} %reduce-scatter.2.cloned.1.call-done) | data formatting | bytes 3145728 | tf_op jit(solution)/shard_map/reshape | solution.py:190
  226.3 3.0 %fusion.16 = bf16[128,2,2048]{2,0,1:T(8,128)(2,1)S(1)} fusion(f32[128,2,2048]{2,1,0:T(2,128)} %reshape.226, f32[2,2048]{1,0:T(2,128)S(1)} %slice.75, bf16[128,2,2048]{2,1,0:T(2,128)(2,1)S(1)} %copy-done.2), kind=kLoop, calls=%fused_computation.28 | loop fusion | flops 2097152 | bytes 4210688 | tf_op jit(solution)/shard_map/convert_element_type | solution.py:192
  229.3 2.0 copy.69
  (66 shorter events, 11.2 us)
Async XLA Ops:
  6.5 169.3 %copy-start = (bf16[256,2048]{1,0:T(8,128)(2,1)S(1)}, bf16[256,2048]{1,0:T(8,128)(2,1)}, u32[]{:S(2)}) copy-start(bf16[256,2048]{1,0:T(8,128)(2,1)} %param.25) | copy-start | bytes 3145732
  6.5 38.9 %copy-start.3 = (bf16[256,2,2048]{2,1,0:T(2,128)(2,1)S(1)}, bf16[256,2,2048]{2,1,0:T(2,128)(2,1)}, u32[]{:S(2)}) copy-start(bf16[256,2,2048]{2,1,0:T(2,128)(2,1)} %param.14) | copy-start | bytes 6291460
  6.5 38.9 %copy-start.6 = (f32[2048]{0:T(1024)S(1)}, f32[2048]{0:T(1024)}, u32[]{:S(2)}) copy-start(f32[2048]{0:T(1024)} %param.20) | copy-start | bytes 24580
  6.5 77.2 %all-gather.5.cloned.1.call-start = ((), (), s32[]{:S(2)}) async-start(), calls=%async_computation.2 | async-start | bytes 1310720 | tf_op jit(solution)/shard_map/all_gather | solution.py:123
  50.0 4.2 %copy-start.4 = (bf16[2048,128]{1,0:T(8,128)(2,1)S(1)}, bf16[2048,128]{1,0:T(8,128)(2,1)}, u32[]{:S(2)}) copy-start(bf16[2048,128]{1,0:T(8,128)(2,1)} %param.23) | copy-start | bytes 1572868
  50.0 7.5 %copy-start.2 = (bf16[128,2,2048]{2,1,0:T(2,128)(2,1)S(1)}, bf16[128,2,2048]{2,1,0:T(2,128)(2,1)}, u32[]{:S(2)}) copy-start(bf16[128,2,2048]{2,1,0:T(2,128)(2,1)} %param.13) | copy-start | bytes 3145732
  57.4 61.8 %all-gather.3.cloned.1.call-start = ((), (), s32[]{:S(2)}) async-start(), calls=%async_computation.1 | async-start | bytes 5242880 | tf_op jit(solution)/shard_map/all_gather | solution.py:92
  57.5 7.4 %copy-start.8 = (f32[4]{0:T(128)S(1)}, f32[4]{0:T(128)}, u32[]{:S(2)}) copy-start(f32[4]{0:T(128)} %param.24) | copy-start | bytes 52
  59.5 163.5 %reduce-scatter.2.cloned.1.call-start = ((), (), s32[]{:S(2)}) async-start(), calls=%async_computation.3 | async-start | bytes 5242880 | tf_op jit(solution)/shard_map/reduce_scatter | solution.py:184
  65.0 77.1 %copy-start.7 = (f32[2,2]{1,0:T(2,128)}, f32[2,2]{1,0:T(2,128)S(1)}, u32[]{:S(2)}) copy-start(f32[2,2]{1,0:T(2,128)S(1)} %max.33) | copy-start | bytes 52
  124.9 14.2 %collective-permute-start.1 = (bf16[128,2,256]{0,2,1:T(8,128)(2,1)S(1)}, bf16[128,2,256]{0,2,1:T(8,128)(2,1)S(1)}, u32[]{:S(2)}, u32[]{:S(2)}) collective-permute-start(bf16[128,2,256]{0,2,1:T(8,128)(2,1)S(1)} %get-tuple-element.41), channel_id=1, source_target_pairs={{4,0},{8,4},{12,8},{5,1},{9,5},{13,9},{6,2},{10,6},{14,10},{7,3},{... | collective-permute-start | bytes 393224 | tf_op jit(solution)/shard_map/ppermute | solution.py:24
  126.2 12.9 %collective-permute-start = (bf16[128,2,256]{0,2,1:T(8,128)(2,1)S(1)}, bf16[128,2,256]{0,2,1:T(8,128)(2,1)S(1)}, u32[]{:S(2)}, u32[]{:S(2)}) collective-permute-start(bf16[128,2,256]{0,2,1:T(8,128)(2,1)S(1)} %get-tuple-element.40), channel_id=1, source_target_pairs={{0,4},{4,8},{8,12},{1,5},{5,9},{9,13},{2,6},{6,10},{10,14},{3,7},{... | collective-permute-start | bytes 393224 | tf_op jit(solution)/shard_map/ppermute | solution.py:22
  142.1 4.5 %copy-start.1 = (f32[2,2,768,512,2]{3,2,4,1,0:T(8,128)}, f32[2,2,768,512,2]{3,2,4,1,0:T(8,128)S(1)}, u32[]{:S(2)}) copy-start(f32[2,2,768,512,2]{3,2,4,1,0:T(8,128)S(1)} %get-tuple-element.47) | copy-start | bytes 37748740
  146.6 18.2 %slice-start = ((s8[12582912]{0:T(1024)(128)(4,1)}), s8[4194304]{0:T(1024)(128)(4,1)S(1)}, s32[]{:S(2)}) async-start(s8[12582912]{0:T(1024)(128)(4,1)} %bitcast.69), calls=%async_computation.4 | async-start | bytes 8388608
  156.7 8.1 %slice-start.1 = ((s8[12582912]{0:T(1024)(128)(4,1)}), s8[4194304]{0:T(1024)(128)(4,1)S(1)}, s32[]{:S(2)}) async-start(s8[12582912]{0:T(1024)(128)(4,1)} %bitcast.69), calls=%async_computation.5 | async-start | bytes 8388608
  156.8 8.5 %slice-start.2 = ((s8[12582912]{0:T(1024)(128)(4,1)}), s8[4194304]{0:T(1024)(128)(4,1)S(1)}, s32[]{:S(2)}) async-start(s8[12582912]{0:T(1024)(128)(4,1)} %bitcast.69), calls=%async_computation.6 | async-start | bytes 8388608
  156.8 8.5 %copy-start.5 = (bf16[768,2,128]{0,2,1:T(8,128)(2,1)S(1)}, bf16[768,2,128]{0,2,1:T(8,128)(2,1)}, u32[]{:S(2)}) copy-start(bf16[768,2,128]{0,2,1:T(8,128)(2,1)} %get-tuple-element.36) | copy-start | bytes 1179652
Sparse Core Ops, SparseCore 0:
  57.5 26.2 all-gather.4
  85.3 33.8 all-gather.2
  179.2 43.6 reduce-scatter.1
where the time goes:
time: 239 us; the launch traced here: 238 us
  waiting for transfers between devices  86.6 us (36%)
  matrix products  37.3 us (16%)
  blocking collectives  36.2 us (15%)
  local copies, waits for them, and re-layouts  30.6 us (13%)
  other arithmetic  27.7 us (12%)
  between operations  13.4 us (6%)
  starting transfers between devices  6.11 us (3%)
    reduce_scatter x1, waiting for transfers between devices, on_device(): lax.psum_scatter(jnp.dot(attended, w_out, preferred_element_type=jnp.floa...  38.6 us
    all_gather x1, waiting for transfers between devices, on_device(): shard_rows = lax.all_gather(normed, 'tp', axis=0, tiled=True)  30.3 us
    psum x1, blocking collectives, on_device(): lax.psum((part_shift, part_scale, part_gate), 'sp')  20.7 us
    all_gather x1, waiting for transfers between devices, on_device(): lax.all_gather(jnp.dot(flat_ctx, w_pair, preferred_element_type=jnp.float...  17.6 us
    reduce_sum x1, other arithmetic, attend_block(): jnp.sum(ctx_exp, axis=-1)  9.31 us
    dot_general x1, matrix products, attend_block(): jnp.einsum('qsngd,ksnd->sngqk', q_blk, ctx_keys, preferred_element_type=j...  8.13 us
    dot_general x1, matrix products, attend_block(): jnp.einsum('sngqk,ksnd->qsngd', ctx_weights, ctx_values, preferred_elemen...  8.03 us
    unnamed x27, local copies, waits for them, and re-layouts  7.63 us
  transfers between devices with their start and end apart: 5, of which 3 were waited for; matrix products, arithmetic and copies ran while one was open for 9% of the time, Pallas kernels for 0%

commit v1 on v0

--- a/solution.py
+++ b/solution.py
@@ -89,7 +89,12 @@
     )
     normed = modulate(latents, norm_gain, shift_all[:samples][None], scale_all[:samples][None])
     w_joint = jnp.concatenate([w_query, w_key, w_value], axis=1)
-    shard_rows = lax.all_gather(normed, "tp", axis=0, tiled=True)
+    ring = [normed]
+    for hop in range(3):
+        ring.append(lax.ppermute(ring[-1], "tp", [(dev, (dev + 1) % 4) for dev in range(4)]))
+    shard_rows = jnp.roll(
+        jnp.concatenate(ring[::-1], axis=0), (lax.axis_index("tp") + 1) * ring[0].shape[0], axis=0
+    )
     row_count = shard_rows.shape[0]
     flat_rows = shard_rows.reshape(row_count * samples, model_width)
     projected = jnp.dot(flat_rows, w_joint, preferred_element_type=jnp.float32).reshape(

time: 239 us -> 220 us (0.921)
  waiting for transfers between devices: 86.6 us -> 60.8 us
  local copies, waits for them, and re-layouts: 30.6 us -> 36.3 us
    all_gather x1 -> x0, waiting for transfers between devices: 30.3 us -> none  [on_device(): shard_rows = lax.all_gather(normed, 'tp', axis=0, tiled=True)]
    ppermute x0 -> x3, waiting for transfers between devices: none -> 8.06 us  [on_device(): lax.ppermute(ring[-1], 'tp', [(dev, (dev + 1) % 4) for dev in range(4)])]
    unnamed x27 -> x53, local copies, waits for them, and re-layouts: 7.63 us -> 14.3 us
    all_gather x1, waiting for transfers between devices: 17.6 us -> 13.8 us  [on_device(): lax.all_gather(jnp.dot(flat_ctx, w_pair, preferred_element_type=jnp.float...]
    dot_general x1, matrix products: 5.16 us -> 2.39 us  [on_device(): jnp.dot(flat_rows, w_joint, preferred_element_type=jnp.float32)]
  transfers between devices with their start and end apart: 5 -> 7, of which waited for: 3 -> 4; matrix products, arithmetic and copies ran while one was open for 9% -> 17% of each run, Pallas kernels for 0% -> 0%
where the time goes in v1:
time: 220 us; the launch traced here: 219 us
  waiting for transfers between devices  60.8 us (28%)
  blocking collectives  36.8 us (17%)
  local copies, waits for them, and re-layouts  36.3 us (16%)
  matrix products  35.7 us (16%)
  other arithmetic  29 us (13%)
  between operations  13.9 us (6%)
  starting transfers between devices  6.47 us (3%)
    reduce_scatter x1, waiting for transfers between devices, on_device(): lax.psum_scatter(jnp.dot(attended, w_out, preferred_element_type=jnp.floa...  38.9 us
    psum x1, blocking collectives, on_device(): lax.psum((part_shift, part_scale, part_gate), 'sp')  21.3 us
    unnamed x53, local copies, waits for them, and re-layouts  14.3 us
    all_gather x1, waiting for transfers between devices, on_device(): lax.all_gather(jnp.dot(flat_ctx, w_pair, preferred_element_type=jnp.float...  13.8 us
    reduce_sum x1, other arithmetic, attend_block(): jnp.sum(ctx_exp, axis=-1)  8.61 us
    dot_general x1, matrix products, attend_block(): jnp.einsum('qsngd,ksnd->sngqk', q_blk, ctx_keys, preferred_element_type=j...  8.13 us
    ppermute x3, waiting for transfers between devices, on_device(): lax.ppermute(ring[-1], 'tp', [(dev, (dev + 1) % 4) for dev in range(4)])  8.06 us
    dot_general x1, matrix products, attend_block(): jnp.einsum('sngqk,ksnd->qsngd', ctx_weights, ctx_values, preferred_elemen...  7.97 us
  transfers between devices with their start and end apart: 7, of which 4 were waited for; matrix products, arithmetic and copies ran while one was open for 17% of the time, Pallas kernels for 0%

profile of v1, /device:TPU:0, one launch (start us, length us, event | category | flops | bytes accessed | tf_op | source)
XLA Modules:
  0.0 219.0 jit_solution(10427119929308640314)
XLA Ops:
  10.5 21.3 %all-reduce = (f32[3,512]{1,0:T(4,128)S(1)}, f32[3,512]{1,0:T(4,128)S(1)}, f32[3,512]{1,0:T(4,128)}) all-reduce(f32[3,512]{1,0:T(4,128)S(1)} %fusion.51, f32[3,512]{1,0:T(4,128)S(1)} %fusion.53, f32[3,512]{1,0:T(4,128)S(1)} %fusion.55), channel_id=1, replica_groups=mesh['grp'=2,'sp'=4,'tp'=4] {'sp'}, use_global_device_ids=true, to_apply=%region_3.4 | all-reduce | flops 4608 | bytes 36864 | tf_op jit(solution)/shard_map/psum | solution.py:84
  31.7 5.2 %all_gather.14 = f32[3,2048]{1,0:T(4,128)S(1)} all-gather(f32[3,512]{1,0:T(4,128)S(1)} %get-tuple-element.19), channel_id=1, replica_groups=mesh['grp'=2,'sp'=4,'tp'=4] {'tp'}, dimensions={1}, use_global_device_ids=true | all-gather | bytes 30720 | tf_op jit(solution)/shard_map/all_gather | solution.py:86
  36.9 5.2 %all_gather.13 = f32[3,2048]{1,0:T(4,128)S(1)} all-gather(f32[3,512]{1,0:T(4,128)S(1)} %get-tuple-element.20), channel_id=1, replica_groups=mesh['grp'=2,'sp'=4,'tp'=4] {'tp'}, dimensions={1}, use_global_device_ids=true | all-gather | bytes 30720 | tf_op jit(solution)/shard_map/all_gather | solution.py:87
  43.7 2.8 %fusion.17 = bf16[128,2,2048]{2,0,1:T(8,128)(2,1)} fusion(f32[2,2048]{1,0:T(2,128)S(1)} %slice.77, f32[2,2048]{1,0:T(2,128)S(1)} %slice_add_fusion, f32[2048]{0:T(1024)} %param.20, f32[128,2]{0,1:T(2,128)S(1)} %add_rsqrt_fusion.1, bf16[128,2,2048]{2,1,0:T(2,128)(2,1)} %param.13), kind=kLoop, calls=%fused_computation.29 | loop fusion | flops 3145728 | bytes 2139136 | tf_op jit(solution)/shard_map/convert_element_type | solution.py:49
  46.9 2.2 %fusion.6 = f32[256,2]{1,0:T(8,128)S(1)} fusion(bf16[256,2,2048]{2,1,0:T(2,128)(2,1)S(1)} %copy-done.4), kind=kLoop, calls=%fused_computation.14 | loop fusion | flops 3145216 | bytes 2099200 | tf_op jit(solution)/shard_map/reduce_sum | solution.py:48
  49.2 4.6 %fusion.10 = bf16[256,2,2048]{2,1,0:T(2,128)(2,1)} fusion(bf16[256,2,2048]{2,1,0:T(2,128)(2,1)S(1)} %copy-done.4, f32[2048]{0:T(1024)S(1)} %bitcast.81, f32[2048]{0:T(1024)S(1)} %bitcast.80, f32[2048]{0:T(1024)S(1)} %copy-done.15, f32[256,2]{1,0:T(8,128)S(1)} %add_rsqrt_fusion), kind=kLoop, calls=%fused_computation.18 | loop fusion | flops 6291456 | bytes 4220928 | tf_op jit(solution)/shard_map/convert_element_type | solution.py:49
  53.8 4.1 %reshape.218 = bf16[512,2048]{1,0:T(8,128)(2,1)} reshape(bf16[256,2,2048]{2,1,0:T(2,128)(2,1)} %fusion.10) | data formatting | bytes 4194304 | tf_op jit(solution)/shard_map/reshape | solution.py:127
  57.9 3.2 %collective-permute-done = bf16[128,2,2048]{2,0,1:T(8,128)(2,1)} collective-permute-done((bf16[128,2,2048]{2,0,1:T(8,128)(2,1)}, bf16[128,2,2048]{2,0,1:T(8,128)(2,1)}, u32[]{:S(2)}, u32[]{:S(2)}) %collective-permute-start) | collective-permute-done | bytes 1048608 | tf_op jit(solution)/shard_map/ppermute | solution.py:94
  61.1 2.5 %convolution_convert_fusion.1 = bf16[512,256]{1,0:T(8,128)(2,1)S(1)} fusion(bf16[512,2048]{1,0:T(8,128)(2,1)} %reshape.218, bf16[2048,128]{1,0:T(8,128)(2,1)} %param.23, bf16[2048,128]{1,0:T(8,128)(2,1)} %param.22), kind=kOutput, calls=%fused_computation.43 | convolution fusion | flops 539099136 | bytes 3407872 | tf_op jit(solution)/shard_map/dot_general | solution.py:129
  64.5 2.0 copy.60
  66.6 2.0 copy.59
  70.7 4.9 %collective-permute-done.1 = bf16[128,2,2048]{2,0,1:T(8,128)(2,1)S(1)} collective-permute-done((bf16[128,2,2048]{2,0,1:T(8,128)(2,1)}, bf16[128,2,2048]{2,0,1:T(8,128)(2,1)S(1)}, u32[]{:S(2)}, u32[]{:S(2)}) %collective-permute-start.1) | collective-permute-done | bytes 1048608 | tf_op jit(solution)/shard_map/ppermute | solution.py:94
  77.3 13.8 %all-gather.2.cloned.1.call-done = bf16[1024,2,256]{2,1,0:T(2,128)(2,1)} async-done(((bf16[256,2,256]{2,1,0:T(2,128)(2,1)}), bf16[1024,2,256]{2,1,0:T(2,128)(2,1)}) %all-gather.2.cloned.1.call-update) | async-done | bytes 1048592 | tf_op jit(solution)/shard_map/all_gather | solution.py:128
  91.1 2.9 %fusion.57 = (bf16[1024,2,128]{2,1,0:T(2,128)(2,1)}, bf16[1024,2,128]{2,1,0:T(2,128)(2,1)}) fusion(bf16[1024,2,256]{2,1,0:T(2,128)(2,1)} %all-gather.2.cloned.1.call-done), kind=kLoop, calls=%fused_computation.108 | loop fusion | bytes 2097152 | tf_op jit(solution)/shard_map/slice | solution.py:137
  94.0 2.1 copy.65
  96.2 2.0 copy.63
  105.1 2.4 %fusion.11 = f32[512,2,512]{0,2,1:T(8,128)S(1)} fusion(bf16[1024,2,2048]{2,0,1:T(8,128)(2,1)S(1)} %constant_dynamic-update-slice_fusion, s32[]{:T(128)S(6)} %select_n.38, bf16[2048,128]{0,1:T(8,128)(2,1)S(1)} %copy-done.10, bf16[2048,128]{0,1:T(8,128)(2,1)S(1)} %copy-done.11, bf16[2048,256]{0,1:T(8,128)(2,1)S(1)} %copy-done.7), kind=kOutput, calls=%fused_computation.19 | convolution fusion | flops 2153775104 | bytes 8388612 | tf_op jit(solution)/shard_map/dot_general | solution.py:100
  109.4 4.8 %collective-permute-start.3 = (bf16[128,2,256]{0,2,1:T(8,128)(2,1)S(1)}, bf16[128,2,256]{0,2,1:T(8,128)(2,1)S(1)}, u32[]{:S(2)}, u32[]{:S(2)}) collective-permute-start(bf16[128,2,256]{0,2,1:T(8,128)(2,1)S(1)} %get-tuple-element.40), channel_id=1, source_target_pairs={{0,4},{4,8},{8,12},{1,5},{5,9},{9,13},{2,6},{6,10},{10,14},{3,7},{... | collective-permute-start | bytes 393224 | tf_op jit(solution)/shard_map/ppermute | solution.py:22
  114.2 8.1 %bitcast_reduce_fusion = (f32[2,2,2,512]{3,2,1,0:T(2,128)S(1)}, f32[2,2,1024,512,2]{3,2,4,1,0:T(8,128)}) fusion(bf16[1024,2,2,64,1]{0,3,4,2,1:T(8,128)(2,1)S(1)} %bitcast.71, bf16[512,2,2,2,32]{0,4,3,2,1:T(8,128)(2,1)S(1)} %bitcast.75, bf16[512,2,2,2,32]{0,4,3,2,1:T(8,128)(2,1)S(1)} %bitcast.73), kind=kOutput, calls=%fused_computation.1 | convolution fusion | flops 546304000 | bytes 17842176 | tf_op jit(solution)/shard_map/while/body/eval_jaxpr/qsngd,ksnd->sngqk/dot_general | solution.py:167
  122.5 2.1 fusion.3
  124.7 2.6 %fusion.2 = f32[2,2,2,512]{3,2,1,0:T(2,128)S(1)} fusion(f32[2,2,768,512,2]{3,2,4,1,0:T(8,128)S(1)} %get-tuple-element.47, f32[2,2,2,512]{3,2,1,0:T(2,128)S(1)} %maximum_maximum_fusion, pred[512,768]{0,1:T(8,128)(4,1)S(1)} %fusion.24), kind=kLoop, calls=%fused_computation.8 | loop fusion | flops 12578816 | bytes 13008896 | tf_op jit(solution)/shard_map/while/body/eval_jaxpr/reduce_sum | solution.py:176
  127.3 1.9 copy-done.2
  129.1 8.6 %fusion.1 = f32[2,2,2,512]{3,2,1,0:T(2,128)S(1)} fusion(f32[2,2,1024,512,2]{3,2,4,1,0:T(8,128)} %get-tuple-element.49, f32[2,2,2,512]{3,2,1,0:T(2,128)S(1)} %maximum_maximum_fusion), kind=kLoop, calls=%fused_computation.4 | loop fusion | flops 12578816 | bytes 16809984 | tf_op jit(solution)/shard_map/while/body/eval_jaxpr/reduce_sum | solution.py:176
  137.9 8.0 %fusion.4 = f32[2,2,64,2,512]{4,2,3,1,0:T(8,128)S(1)} fusion(bf16[1024,2,2,64,1]{0,3,4,2,1:T(8,128)(2,1)S(1)} %bitcast.77, f32[2,2,1024,512,2]{3,2,4,1,0:T(8,128)} %get-tuple-element.49, f32[2,2,2,512]{3,2,1,0:T(2,128)S(1)} %exponential_add_fusion, f32[2,2,2,512]{3,2,1,0:T(2,128)S(1)} %maximum_maximum_fusion), kind=kOutput, calls=%fused_computation.10 | convolution fusion | flops 553648128 | bytes 18382848 | tf_op jit(solution)/shard_map/while/body/eval_jaxpr/sngqk,ksnd->qsngd/dot_general | solution.py:183
  147.2 4.3 %fusion.27 = bf16[512,2,2,2,64]{0,4,3,2,1:T(8,128)(2,1)} fusion(f32[2,2,64,2,512]{4,2,3,1,0:T(8,128)S(1)} %fusion.4, bf16[768,2,2,64,1]{0,3,4,2,1:T(8,128)(2,1)S(1)} %bitcast.78, f32[2,2,768,512,2]{3,2,4,1,0:T(8,128)S(1)} %copy-done.3, f32[2,2,2,512]{3,2,1,0:T(2,128)S(1)} %exponential_add_fusion, f32[2,2,2,512]{3,2,1,0:T(2,128)S(1)} %maximum_maximum_fusion, ...), kind=kOutput, calls=%fused_computation.42 | convolution fusion | flops 418906112 | bytes 14974976 | tf_op jit(solution)/shard_map/while/body/eval_jaxpr/sngqk,ksnd->qsngd/dot_general | solution.py:180
  151.5 2.4 %copy.67 = bf16[512,2,2,2,64]{4,3,2,1,0:T(2,128)(2,1)S(1)} copy(bf16[512,2,2,2,64]{0,4,3,2,1:T(8,128)(2,1)} %fusion.27) | data formatting | bytes 1048576 | tf_op jit(solution)/shard_map/while/body/eval_jaxpr/convert_element_type | solution.py:186
  155.4 4.3 %convolution_convert_fusion = bf16[1024,2048]{1,0:T(8,128)(2,1)} fusion(bf16[1024,256]{1,0:T(8,128)(2,1)} %reshape.222, bf16[256,2048]{1,0:T(8,128)(2,1)S(1)} %copy-done), kind=kOutput, calls=%fused_computation.21 | convolution fusion | flops 1075838976 | bytes 5767168 | tf_op jit(solution)/shard_map/dot_general | solution.py:190
  159.7 5.2 %all_gather.12 = f32[3,2048]{1,0:T(4,128)S(1)} all-gather(f32[3,512]{1,0:T(4,128)S(1)} %copy-done.19), channel_id=1, replica_groups=mesh['grp'=2,'sp'=4,'tp'=4] {'tp'}, dimensions={1}, use_global_device_ids=true | all-gather | bytes 30720 | tf_op jit(solution)/shard_map/all_gather | solution.py:88
  164.9 38.9 %reduce-scatter.2.cloned.1.call-done = bf16[256,2048]{1,0:T(8,128)(2,1)} async-done(((bf16[1024,2048]{1,0:T(8,128)(2,1)}), bf16[256,2048]{1,0:T(8,128)(2,1)}) %reduce-scatter.2.cloned.1.call-update) | async-done | bytes 1048592 | tf_op jit(solution)/shard_map/reduce_scatter | solution.py:189
  203.7 3.3 %reshape.226 = f32[128,2,2048]{2,1,0:T(2,128)} reshape(bf16[256,2048]{1,0:T(8,128)(2,1)} %reduce-scatter.2.cloned.1.call-done) | data formatting | bytes 3145728 | tf_op jit(solution)/shard_map/reshape | solution.py:195
  207.1 3.0 %fusion.18 = bf16[128,2,2048]{2,0,1:T(8,128)(2,1)S(1)} fusion(f32[128,2,2048]{2,1,0:T(2,128)} %reshape.226, f32[2,2048]{1,0:T(2,128)S(1)} %slice.75, bf16[128,2,2048]{2,1,0:T(2,128)(2,1)S(1)} %copy-done.1), kind=kLoop, calls=%fused_computation.30 | loop fusion | flops 2097152 | bytes 4210688 | tf_op jit(solution)/shard_map/convert_element_type | solution.py:197
  210.1 2.0 copy.69
  (96 shorter events, 22.3 us)
Async XLA Ops:
  6.5 148.8 %copy-start = (bf16[256,2048]{1,0:T(8,128)(2,1)S(1)}, bf16[256,2048]{1,0:T(8,128)(2,1)}, u32[]{:S(2)}) copy-start(bf16[256,2048]{1,0:T(8,128)(2,1)} %param.25) | copy-start | bytes 3145732
  6.5 42.7 %copy-start.15 = (f32[2048]{0:T(1024)S(1)}, f32[2048]{0:T(1024)}, u32[]{:S(2)}) copy-start(f32[2048]{0:T(1024)} %param.20) | copy-start | bytes 24580
  6.5 40.4 %copy-start.4 = (bf16[256,2,2048]{2,1,0:T(2,128)(2,1)S(1)}, bf16[256,2,2048]{2,1,0:T(2,128)(2,1)}, u32[]{:S(2)}) copy-start(bf16[256,2,2048]{2,1,0:T(2,128)(2,1)} %param.14) | copy-start | bytes 6291460
  6.5 84.6 %all-gather.2.cloned.1.call-start = ((), (), s32[]{:S(2)}) async-start(), calls=%async_computation.1 | async-start | bytes 1310720 | tf_op jit(solution)/shard_map/all_gather | solution.py:128
  42.1 11.7 %copy-start.13 = (f32[2,2048]{1,0:T(2,128)}, f32[2,2048]{1,0:T(2,128)S(1)}, u32[]{:S(2)}) copy-start(f32[2,2048]{1,0:T(2,128)S(1)} %slice_add_fusion) | copy-start | bytes 49156
  43.7 3.2 %copy-start.17 = (f32[128,2]{0,1:T(2,128)}, f32[128,2]{0,1:T(2,128)S(1)}, u32[]{:S(2)}) copy-start(f32[128,2]{0,1:T(2,128)S(1)} %add_rsqrt_fusion.1) | copy-start | bytes 3076
  46.6 14.5 %collective-permute-start = (bf16[128,2,2048]{2,0,1:T(8,128)(2,1)}, bf16[128,2,2048]{2,0,1:T(8,128)(2,1)}, u32[]{:S(2)}, u32[]{:S(2)}) collective-permute-start(bf16[128,2,2048]{2,0,1:T(8,128)(2,1)} %fusion.17), channel_id=1, source_target_pairs={{0,1},{1,2},{2,3},{3,0},{4,5},{5,6},{6,7},{7,4},{8,9},{9,10},{10,1... | collective-permute-start | bytes 3145736 | tf_op jit(solution)/shard_map/ppermute | solution.py:94
  57.9 10.7 %copy-start.6 = (bf16[2048,256]{1,0:T(8,128)(2,1)S(1)}, bf16[2048,256]{1,0:T(8,128)(2,1)}, u32[]{:S(2)}) copy-start(bf16[2048,256]{1,0:T(8,128)(2,1)} %param.21) | copy-start | bytes 3145732
  57.9 12.1 %copy-start.21 = (f32[4]{0:T(128)S(1)}, f32[4]{0:T(128)}, u32[]{:S(2)}) copy-start(f32[4]{0:T(128)} %param.24) | copy-start | bytes 52
  61.1 14.4 %collective-permute-start.1 = (bf16[128,2,2048]{2,0,1:T(8,128)(2,1)}, bf16[128,2,2048]{2,0,1:T(8,128)(2,1)S(1)}, u32[]{:S(2)}, u32[]{:S(2)}) collective-permute-start(bf16[128,2,2048]{2,0,1:T(8,128)(2,1)} %collective-permute-done), channel_id=1, source_target_pairs={{0,1},{1,2},{2,3},{3,0},{4,5},{5,6},{6,7},{7,4},{8,9},{9,10},{10,1... | collective-permute-start | bytes 3145736 | tf_op jit(solution)/shard_map/ppermute | solution.py:94
  64.5 139.3 %reduce-scatter.2.cloned.1.call-start = ((), (), s32[]{:S(2)}) async-start(), calls=%async_computation.2 | async-start | bytes 5242880 | tf_op jit(solution)/shard_map/reduce_scatter | solution.py:189
  75.5 22.7 %collective-permute-start.2 = (bf16[128,2,2048]{2,0,1:T(8,128)(2,1)S(1)}, bf16[128,2,2048]{2,0,1:T(8,128)(2,1)}, u32[]{:S(2)}, u32[]{:S(2)}) collective-permute-start(bf16[128,2,2048]{2,0,1:T(8,128)(2,1)S(1)} %collective-permute-done.1), channel_id=1, source_target_pairs={{0,1},{1,2},{2,3},{3,0},{4,5},{5,6},{6,7},{7,4},{8,9},{9,10},{10,1... | collective-permute-start | bytes 3145736 | tf_op jit(solution)/shard_map/ppermute | solution.py:94
  94.0 6.9 %copy-start.1 = (bf16[128,2,2048]{2,1,0:T(2,128)(2,1)S(1)}, bf16[128,2,2048]{2,1,0:T(2,128)(2,1)}, u32[]{:S(2)}) copy-start(bf16[128,2,2048]{2,1,0:T(2,128)(2,1)} %param.13) | copy-start | bytes 3145732
  98.2 2.8 %copy-start.14 = (f32[2,2048]{1,0:T(2,128)S(1)}, f32[2,2048]{1,0:T(2,128)}, u32[]{:S(2)}) copy-start(f32[2,2048]{1,0:T(2,128)} %copy-done.13) | copy-start | bytes 49156
  98.2 2.8 %copy-start.16 = (f32[2048]{0:T(1024)S(1)}, f32[2048]{0:T(1024)}, u32[]{:S(2)}) copy-start(f32[2048]{0:T(1024)} %param.20) | copy-start | bytes 24580
  98.2 2.8 %copy-start.18 = (f32[128,2]{0,1:T(2,128)S(1)}, f32[128,2]{0,1:T(2,128)}, u32[]{:S(2)}) copy-start(f32[128,2]{0,1:T(2,128)} %copy-done.17) | copy-start | bytes 3076
  101.6 3.5 %copy-start.7 = (bf16[2048,256]{0,1:T(8,128)(2,1)S(1)}, bf16[2048,256]{0,1:T(8,128)(2,1)}, u32[]{:S(2)}) copy-start(bf16[2048,256]{0,1:T(8,128)(2,1)} %copy.58) | copy-start | bytes 3145732
  101.6 3.5 %copy-start.10 = (bf16[2048,128]{0,1:T(8,128)(2,1)S(1)}, bf16[2048,128]{0,1:T(8,128)(2,1)}, u32[]{:S(2)}) copy-start(bf16[2048,128]{0,1:T(8,128)(2,1)} %copy.60) | copy-start | bytes 1572868
  101.6 3.5 %copy-start.11 = (bf16[2048,128]{0,1:T(8,128)(2,1)S(1)}, bf16[2048,128]{0,1:T(8,128)(2,1)}, u32[]{:S(2)}) copy-start(bf16[2048,128]{0,1:T(8,128)(2,1)} %copy.59) | copy-start | bytes 1572868
  105.1 2.6 %copy-start.8 = (f32[512,32]{0,1:T(8,128)S(1)}, f32[512,32]{0,1:T(8,128)}, u32[]{:S(2)}) copy-start(f32[512,32]{0,1:T(8,128)} %get-tuple-element.42) | copy-start | bytes 196612
  105.1 2.6 %copy-start.9 = (f32[512,32]{0,1:T(8,128)S(1)}, f32[512,32]{0,1:T(8,128)}, u32[]{:S(2)}) copy-start(f32[512,32]{0,1:T(8,128)} %get-tuple-element.43) | copy-start | bytes 196612
  107.5 6.6 %copy-start.5 = (bf16[1024,2,128]{0,2,1:T(8,128)(2,1)S(1)}, bf16[1024,2,128]{0,2,1:T(8,128)(2,1)}, u32[]{:S(2)}) copy-start(bf16[1024,2,128]{0,2,1:T(8,128)(2,1)} %copy.63) | copy-start | bytes 1572868
  108.1 14.2 %collective-permute-start.4 = (bf16[128,2,256]{0,2,1:T(8,128)(2,1)S(1)}, bf16[128,2,256]{0,2,1:T(8,128)(2,1)S(1)}, u32[]{:S(2)}, u32[]{:S(2)}) collective-permute-start(bf16[128,2,256]{0,2,1:T(8,128)(2,1)S(1)} %get-tuple-element.41), channel_id=1, source_target_pairs={{4,0},{8,4},{12,8},{5,1},{9,5},{13,9},{6,2},{10,6},{14,10},{7,3},{... | collective-permute-start | bytes 393224 | tf_op jit(solution)/shard_map/ppermute | solution.py:24
  109.4 12.9 %collective-permute-start.3 = (bf16[128,2,256]{0,2,1:T(8,128)(2,1)S(1)}, bf16[128,2,256]{0,2,1:T(8,128)(2,1)S(1)}, u32[]{:S(2)}, u32[]{:S(2)}) collective-permute-start(bf16[128,2,256]{0,2,1:T(8,128)(2,1)S(1)} %get-tuple-element.40), channel_id=1, source_target_pairs={{0,4},{4,8},{8,12},{1,5},{5,9},{9,13},{2,6},{6,10},{10,14},{3,7},{... | collective-permute-start | bytes 393224 | tf_op jit(solution)/shard_map/ppermute | solution.py:22
  122.4 2.2 copy-start.20
  124.6 4.5 %copy-start.2 = (f32[2,2,768,512,2]{3,2,4,1,0:T(8,128)}, f32[2,2,768,512,2]{3,2,4,1,0:T(8,128)S(1)}, u32[]{:S(2)}) copy-start(f32[2,2,768,512,2]{3,2,4,1,0:T(8,128)S(1)} %get-tuple-element.47) | copy-start | bytes 37748740
  129.1 8.7 %copy-start.12 = (bf16[1024,2,128]{0,2,1:T(8,128)(2,1)S(1)}, bf16[1024,2,128]{0,2,1:T(8,128)(2,1)}, u32[]{:S(2)}) copy-start(bf16[1024,2,128]{0,2,1:T(8,128)(2,1)} %copy.65) | copy-start | bytes 1572868
  137.8 9.3 %copy-start.3 = (f32[2,2,768,512,2]{3,2,4,1,0:T(8,128)S(1)}, f32[2,2,768,512,2]{3,2,4,1,0:T(8,128)}, u32[]{:S(2)}) copy-start(f32[2,2,768,512,2]{3,2,4,1,0:T(8,128)} %copy-done.2) | copy-start | bytes 37748740
  155.4 4.3 %copy-start.19 = (f32[3,512]{1,0:T(4,128)S(1)}, f32[3,512]{1,0:T(4,128)}, u32[]{:S(2)}) copy-start(f32[3,512]{1,0:T(4,128)} %get-tuple-element.21) | copy-start | bytes 18436
Sparse Core Ops, SparseCore 0:
  64.6 26.5 all-gather.1
  159.8 43.9 reduce-scatter.1
